TPU v7x, 32 devices: a whole 2x2x4 slice. The times are simulated.
32 devices in a mesh: rep: 2 (over x), fs: 8 (over z, y), tp: 2 (over core).
Axes of the slice: x: 2, y: 2, z: 4, core: 2. Of those that a mesh axis runs over, the one named last changes fastest.
Arguments:
- inputs: bfloat16 [8192, 1024], P(('rep', 'fs', 'tp')), may hold values from -6 to 6
- up_proj: bfloat16 [1024, 4096], P('fs', 'tp'), may hold values from -0.1875 to 0.1875
- down_proj: bfloat16 [4096, 1024], P('tp', 'fs'), may hold values from -0.09375 to 0.09375
- out_cotangent: bfloat16 [8192, 1024], P(('rep', 'fs', 'tp')), may hold values from -6 to 6
Outputs:
- grad_inputs: bfloat16 [8192, 1024], P(('rep', 'fs', 'tp'))
- grad_up: float32 [1024, 4096], P('fs', 'tp')
- grad_down: float32 [4096, 1024], P('tp', 'fs')
- energy_up: float32 [1024], P('fs')
- energy_down: float32 [4096], P('tp')
All inputs are finite; a program needn't handle non-finite values.
Results may differ from a plain program's by a relative error of at most 0.001.
Values may be sent and summed in bfloat16 or wider, within the bound.
A program may use at most 128 MiB of HBM per device.

v0:
```python
import jax
import jax.numpy as jnp
from jax import lax
from jax.sharding import PartitionSpec as P

D = 1024
FF = 4096


def taken_in(shard, axis, dim, absorb, state):
    everything = jax.tree.map(lambda a: lax.all_gather(a, axis, axis=dim, tiled=True), shard)
    return absorb(state, everything, jnp.int32(0))


def summed_rows(product, span, axis):
    whole = product(jnp.int32(0), span * lax.axis_size(axis))
    return lax.psum_scatter(whole, axis, scatter_dimension=0, tiled=True)


def contract(left, right, left_dim, right_dim):
    return lax.dot_general(
        left, right, (((left_dim,), (right_dim,)), ((), ())), preferred_element_type=jnp.float32
    )


def body(inputs, up_proj, down_proj, out_cotangent):
    factor = float(
        inputs.shape[0] * lax.axis_size("rep") * lax.axis_size("fs") * lax.axis_size("tp")
    ) ** (-0.5)
    all_inputs, all_cotangent = (
        lax.all_gather(inputs, "tp", axis=0, tiled=True),
        lax.all_gather(out_cotangent, "tp", axis=0, tiled=True),
    )
    hidden_cols = up_proj.shape[1]
    group_rows = all_inputs.shape[0]
    whole_up = lax.all_gather(up_proj, "fs", axis=0, tiled=True)
    pre = jnp.dot(all_inputs, whole_up, preferred_element_type=jnp.float32)
    active = jnp.square(jax.nn.relu(pre)).astype(jnp.bfloat16)

    def add_cols(total, piece, start):
        columns = lax.dynamic_slice_in_dim(all_cotangent, start, piece.shape[1], 1)
        return total + contract(columns, piece, 1, 1)

    back = taken_in(down_proj, "fs", 1, add_cols, jnp.zeros((group_rows, hidden_cols), jnp.float32))
    grad_pre = (2.0 * jax.nn.relu(pre) * back).astype(jnp.bfloat16)

    def input_part(start, count):
        rows = lax.dynamic_slice_in_dim(grad_pre, start, count, 0)
        return contract(rows, whole_up, 1, 1)

    grad_inputs = summed_rows(input_part, inputs.shape[0], "tp")
    grad_inputs = grad_inputs.astype(jnp.bfloat16)
    shard_rows = up_proj.shape[0]

    def up_part(start, count):
        columns = lax.dynamic_slice_in_dim(all_inputs, start, count, 1)
        return contract(columns, grad_pre, 0, 0) * factor

    def down_part(start, count):
        columns = lax.dynamic_slice_in_dim(all_cotangent, start, count, 1)
        return contract(columns, active, 0, 0) * factor

    def joint_part(start, count):
        return jnp.concatenate([up_part(start, count), down_part(start, count)], axis=1)

    joint_local = summed_rows(joint_part, shard_rows, "fs")
    joint_sum = lax.psum(joint_local, "rep")
    grad_up = joint_sum[:, :hidden_cols]
    down_flip = joint_sum[:, hidden_cols:]
    grad_down = jnp.transpose(down_flip)
    energy_up = lax.psum(jnp.sum(grad_up * grad_up, axis=1), "tp") / FF
    energy_down = lax.psum(jnp.sum(grad_down * grad_down, axis=1), "fs") / D
    return (grad_inputs, grad_up, grad_down, energy_up, energy_down)


def solution(mesh):
    return jax.shard_map(
        body,
        mesh=mesh,
        in_specs=(
            P(("rep", "fs", "tp"), None),
            P("fs", "tp"),
            P("tp", "fs"),
            P(("rep", "fs", "tp"), None),
        ),
        out_specs=(P(("rep", "fs", "tp"), None), P("fs", "tp"), P("tp", "fs"), P("fs"), P("tp")),
        check_vma=False,
    )
```

profile of v0, /device:TPU:0, one launch (start us, length us, event | category | flops | bytes accessed | tf_op | source)
XLA Modules:
  0.0 594.2 jit_solution(6875754057752719887)
XLA Ops:
  7.2 0.0 all-gather.5.cloned.1.call-start
  7.2 0.7 all-gather.5.cloned.1.call-update
  7.9 0.0 all-gather.7.cloned.1.call-start
  7.9 0.7 all-gather.7.cloned.1.call-update
  8.6 0.0 all-gather.9.cloned.1.call-start
  8.7 0.7 all-gather.9.cloned.1.call-update
  9.4 0.0 all-gather.11.cloned.1.call-start
  9.4 0.5 all-gather.11.cloned.1.call-update
  10.0 0.0 reduce-scatter.5.cloned.1.call-start
  10.0 11.3 %all-gather.5.cloned.1.call-done = bf16[512,1024]{1,0:T(8,128)(2,1)} async-done(((bf16[256,1024]{1,0:T(8,128)(2,1)}), bf16[512,1024]{1,0:T(8,128)(2,1)}) %all-gather.5.cloned.1.call-update) | async-done | bytes 1048592 | tf_op jit(solution)/shard_map/all_gather | solution.py:31
  21.3 76.1 %all-gather.7.cloned.1.call-done = bf16[1024,2048]{1,0:T(8,128)(2,1)} async-done(((bf16[128,2048]{1,0:T(8,128)(2,1)}), bf16[1024,2048]{1,0:T(8,128)(2,1)}) %all-gather.7.cloned.1.call-update) | async-done | bytes 4194320 | tf_op jit(solution)/shard_map/all_gather | solution.py:36
  97.4 6.8 %fusion.2 = f32[512,2048]{1,0:T(8,128)} fusion(bf16[512,1024]{1,0:T(8,128)(2,1)} %all-gather.5.cloned.1.call-done, bf16[1024,2048]{1,0:T(8,128)(2,1)} %all-gather.7.cloned.1.call-done), kind=kOutput, calls=%fused_computation.12 | convolution fusion | flops 2147483648 | bytes 9437184 | tf_op jit(solution)/shard_map/dot_general | solution.py:37
  104.2 2.4 all-gather.9.cloned.1.call-done
  106.6 0.0 copy-start.1
  106.6 8.2 %multiply_bitcast_fusion = f32[1024,2048]{0,1:T(8,128)} fusion(bf16[512,1024]{1,0:T(8,128)(2,1)} %all-gather.9.cloned.1.call-done, f32[512,2048]{1,0:T(8,128)} %fusion.2), kind=kOutput, calls=%fused_computation.1 | convolution fusion | flops 2152726528 | bytes 13631488 | tf_op jit(solution)/shard_map/dot_general | solution.py:21
  114.8 0.0 copy-start.2
  114.8 69.5 %all-gather.11.cloned.1.call-done = bf16[2048,1024]{1,0:T(8,128)(2,1)} async-done(((bf16[2048,128]{1,0:T(8,128)(2,1)}), bf16[2048,1024]{1,0:T(8,128)(2,1)}) %all-gather.11.cloned.1.call-update) | async-done | bytes 4194320 | tf_op jit(solution)/shard_map/all_gather | solution.py:11
  184.3 0.0 copy-done.1
  184.3 5.9 multiply_convert_fusion.1
  190.2 0.0 copy-done.2
  190.2 0.0 copy-start.3
  190.2 0.0 copy-start
  190.2 2.4 multiply_bitcast_fusion.1
  192.6 0.0 copy-done.3
  192.6 1.7 copy-done
  194.3 6.4 %pad_maximum_fusion = f32[1024,4096]{0,1:T(8,128)} fusion(f32[1024,2048]{0,1:T(8,128)S(1)} %copy-done, f32[1024,2048]{0,1:T(8,128)S(1)} %multiply_bitcast_fusion.1), kind=kLoop, calls=%fused_computation | loop fusion | flops 4194304 | bytes 33554432 | tf_op jit(solution)/shard_map/concatenate | solution.py:64
  200.7 0.0 copy-start.4
  200.7 0.0 reduce-scatter.5.cloned.1.call-update
  200.8 0.0 reduce-scatter.3.cloned.1.call-start
  200.8 1.5 copy-done.4
  202.3 5.9 fusion.3
  208.2 0.0 reduce-scatter.3.cloned.1.call-update
  208.3 0.0 all-reduce.2.cloned.1.call-start
  208.3 271.0 %reduce-scatter.5.cloned.1.call-done = f32[128,4096]{0,1:T(8,128)} async-done(((f32[1024,4096]{0,1:T(8,128)}), f32[128,4096]{0,1:T(8,128)}) %reduce-scatter.5.cloned.1.call-update) | async-done | bytes 2097168 | tf_op jit(solution)/shard_map/reduce_scatter | solution.py:17
  479.3 0.0 all-reduce.2.cloned.1.call-update
  479.4 11.0 %reduce-scatter.3.cloned.1.call-done = f32[256,1024]{1,0:T(8,128)} async-done(((f32[512,1024]{1,0:T(8,128)}), f32[256,1024]{1,0:T(8,128)}) %reduce-scatter.3.cloned.1.call-update) | async-done | bytes 1048592 | tf_op jit(solution)/shard_map/reduce_scatter | solution.py:17
  490.3 2.1 convert_element_type.10
  492.4 64.5 %all-reduce.2.cloned.1.call-done = f32[128,4096]{0,1:T(8,128)} async-done(((f32[128,4096]{0,1:T(8,128)}), f32[128,4096]{0,1:T(8,128)}) %all-reduce.2.cloned.1.call-update) | async-done | bytes 2097168 | tf_op jit(solution)/shard_map/psum | solution.py:67
  556.9 2.4 multiply_reduce_fusion
  559.3 21.7 %psum.23 = f32[2048]{0:T(1024)S(1)} all-reduce(f32[2048]{0:T(1024)S(1)} %get-tuple-element.10), channel_id=1, replica_groups=mesh['rep'=2,'fs'=8,'tp'=2] {'fs'}, use_global_device_ids=true, to_apply=%region_6.7 | all-reduce | flops 2048 | bytes 16384 | tf_op jit(solution)/shard_map/psum | solution.py:72
  581.0 0.6 broadcast_multiply_fusion
  581.6 1.5 multiply_reduce_fusion.1
  583.1 2.5 psum.22
  585.6 0.5 broadcast_multiply_fusion.1
  586.1 1.3 copy.9
Async XLA Ops:
  7.2 14.1 %all-gather.5.cloned.1.call-start = ((), (), s32[]{:S(2)}) async-start(), calls=%async_computation.2 | async-start | bytes 1572864 | tf_op jit(solution)/shard_map/all_gather | solution.py:31
  7.9 89.5 %all-gather.7.cloned.1.call-start = ((), (), s32[]{:S(2)}) async-start(), calls=%async_computation.3 | async-start | bytes 4718592 | tf_op jit(solution)/shard_map/all_gather | solution.py:36
  8.6 97.9 %all-gather.9.cloned.1.call-start = ((), (), s32[]{:S(2)}) async-start(), calls=%async_computation.4 | async-start | bytes 1572864 | tf_op jit(solution)/shard_map/all_gather | solution.py:32
  9.4 174.9 %all-gather.11.cloned.1.call-start = ((), (), s32[]{:S(2)}) async-start(), calls=%async_computation.5 | async-start | bytes 4718592 | tf_op jit(solution)/shard_map/all_gather | solution.py:11
  10.0 469.4 %reduce-scatter.5.cloned.1.call-start = ((), (), s32[]{:S(2)}) async-start(), calls=%async_computation.7 | async-start | bytes 18874368 | tf_op jit(solution)/shard_map/reduce_scatter | solution.py:17
  106.6 77.7 %copy-start.1 = (bf16[512,1024]{1,0:T(8,128)(2,1)S(1)}, bf16[512,1024]{1,0:T(8,128)(2,1)}, u32[]{:S(2)}) copy-start(bf16[512,1024]{1,0:T(8,128)(2,1)} %all-gather.9.cloned.1.call-done) | copy-start | bytes 3145732
  114.8 75.4 %copy-start.2 = (bf16[512,1024]{1,0:T(8,128)(2,1)S(1)}, bf16[512,1024]{1,0:T(8,128)(2,1)}, u32[]{:S(2)}) copy-start(bf16[512,1024]{1,0:T(8,128)(2,1)} %all-gather.5.cloned.1.call-done) | copy-start | bytes 3145732
  190.2 2.4 copy-start.3
  190.2 4.1 copy-start
  200.7 1.6 copy-start.4
  200.8 289.6 %reduce-scatter.3.cloned.1.call-start = ((), (), s32[]{:S(2)}) async-start(), calls=%async_computation.6 | async-start | bytes 3145728 | tf_op jit(solution)/shard_map/reduce_scatter | solution.py:17
  208.3 348.7 %all-reduce.2.cloned.1.call-start = ((), (), s32[]{:S(2)}) async-start(), calls=%async_computation.8 | async-start | bytes 4194304 | tf_op jit(solution)/shard_map/psum | solution.py:67
Sparse Core Ops, SparseCore 0:
  9.5 11.7 all-gather.4
  23.4 73.9 all-gather.6
  99.0 7.5 all-gather.8
  108.5 75.7 all-gather.10
  200.9 278.4 reduce-scatter.4
  481.4 8.8 reduce-scatter.2
  492.6 64.2 all-reduce.1
where the time goes:
time: 595 us; the launch traced here: 594 us
  waiting for transfers between devices  508 us (85%)
  matrix products  29.2 us (5%)
  blocking collectives  24.1 us (4%)
  between operations  14.2 us (2%)
  other arithmetic  13.5 us (2%)
    reduce_scatter x2, waiting for transfers between devices, summed_rows(): return lax.psum_scatter(whole, axis, scatter_dimension=0, tiled=True)  282 us
    all_gather x1, waiting for transfers between devices, body(): whole_up = lax.all_gather(up_proj, 'fs', axis=0, tiled=True)  76.1 us
    all_gather x1, waiting for transfers between devices, taken_in(): lax.all_gather(a, axis, axis=dim, tiled=True)  69.5 us
    psum x1, waiting for transfers between devices, body(): joint_sum = lax.psum(joint_local, 'rep')  64.5 us
    dot_general x4, matrix products, contract(): lax.dot_general(left, right, (((left_dim,), (right_dim,)), ((), ())), pre...  22.4 us
    psum x1, blocking collectives, body(): energy_down = lax.psum(jnp.sum(grad_down * grad_down, axis=1), 'fs') / D  21.7 us
  transfers between devices with their start and end apart: 7, of which 7 were waited for; matrix products, arithmetic and copies ran while one was open for 4% of the time, Pallas kernels for 0%

commit v1 on v0

--- a/solution.py
+++ b/solution.py
@@ -33,7 +33,14 @@
     )
     hidden_cols = up_proj.shape[1]
     group_rows = all_inputs.shape[0]
-    whole_up = lax.all_gather(up_proj, "fs", axis=0, tiled=True)
+    ways = lax.axis_size("fs")
+    pieces = [up_proj]
+    for far in range(1, ways):
+        pieces.append(
+            lax.ppermute(pieces[far - 1], "fs", [(d, (d - 1) % ways) for d in range(ways)])
+        )
+    line = jnp.concatenate(pieces, axis=0)
+    whole_up = jnp.roll(line, lax.axis_index("fs") * up_proj.shape[0], axis=0)
     pre = jnp.dot(all_inputs, whole_up, preferred_element_type=jnp.float32)
     active = jnp.square(jax.nn.relu(pre)).astype(jnp.bfloat16)
 

time: 595 us -> 594 us (level)
  waiting for transfers between devices: 508 us -> 455 us
  starting transfers between devices: 0.27 us -> 37.5 us
  local copies, waits for them, and re-layouts: 4.54 us -> 19.5 us
    ppermute x0 -> x7, waiting for transfers between devices: none -> 103 us  [body(): lax.ppermute(pieces[far - 1], 'fs', [(d, (d - 1) % ways) for d in range(w...]
    all_gather x1 -> x0, waiting for transfers between devices: 76.1 us -> none  [body(): whole_up = lax.all_gather(up_proj, 'fs', axis=0, tiled=True)]
    all_gather x1, waiting for transfers between devices: 69.5 us -> 0.01 us  [taken_in(): lax.all_gather(a, axis, axis=dim, tiled=True)]
    ppermute x0 -> x7, starting transfers between devices: none -> 37.1 us  [body(): lax.ppermute(pieces[far - 1], 'fs', [(d, (d - 1) % ways) for d in range(w...]
    unnamed x11 -> x28, local copies, waits for them, and re-layouts: 4.54 us -> 18.6 us
    all_gather x1, waiting for transfers between devices: 11.3 us -> 0.01 us  [body(): lax.all_gather(inputs, 'tp', axis=0, tiled=True)]
  transfers between devices with their start and end apart: 7 -> 13, of which waited for: 7 -> 10; matrix products, arithmetic and copies ran while one was open for 4% -> 6% of each run, Pallas kernels for 0% -> 0%
where the time goes in v1:
time: 594 us; the launch traced here: 593 us
  waiting for transfers between devices  455 us (77%)
  starting transfers between devices  37.5 us (6%)
  matrix products  29.2 us (5%)
  blocking collectives  24.1 us (4%)
  local copies, waits for them, and re-layouts  19.5 us (3%)
  between operations  14.2 us (2%)
  other arithmetic  13.5 us (2%)
    reduce_scatter x2, waiting for transfers between devices, summed_rows(): return lax.psum_scatter(whole, axis, scatter_dimension=0, tiled=True)  286 us
    ppermute x7, waiting for transfers between devices, body(): lax.ppermute(pieces[far - 1], 'fs', [(d, (d - 1) % ways) for d in range(w...  103 us
    psum x1, waiting for transfers between devices, body(): joint_sum = lax.psum(joint_local, 'rep')  64.3 us
    ppermute x7, starting transfers between devices, body(): lax.ppermute(pieces[far - 1], 'fs', [(d, (d - 1) % ways) for d in range(w...  37.1 us
    dot_general x4, matrix products, contract(): lax.dot_general(left, right, (((left_dim,), (right_dim,)), ((), ())), pre...  22.4 us
    psum x1, blocking collectives, body(): energy_down = lax.psum(jnp.sum(grad_down * grad_down, axis=1), 'fs') / D  21.7 us
    unnamed x28, local copies, waits for them, and re-layouts  18.6 us
  transfers between devices with their start and end apart: 13, of which 10 were waited for; matrix products, arithmetic and copies ran while one was open for 6% of the time, Pallas kernels for 0%

profile of v1, /device:TPU:0, one launch (start us, length us, event | category | flops | bytes accessed | tf_op | source)
XLA Modules:
  0.0 593.1 jit_solution(229082176077833551)
XLA Ops:
  7.2 0.0 all-gather.4.cloned.1.call-start
  7.2 0.7 all-gather.4.cloned.1.call-update
  7.9 0.0 all-gather.6.cloned.1.call-start
  8.0 0.7 all-gather.6.cloned.1.call-update
  8.7 0.0 all-gather.8.cloned.1.call-start
  8.7 0.7 all-gather.8.cloned.1.call-update
  9.4 0.0 reduce-scatter.5.cloned.1.call-start
  9.4 6.1 %collective-permute-start = (bf16[128,2048]{1,0:T(8,128)(2,1)}, bf16[128,2048]{1,0:T(8,128)(2,1)S(1)}, u32[]{:S(2)}, u32[]{:S(2)}) collective-permute-start(bf16[128,2048]{1,0:T(8,128)(2,1)} %param.5), channel_id=1, source_target_pairs={{0,14},{2,0},{4,2},{6,4},{8,6},{10,8},{12,10},{14,12},{1,15},{3,1}... | collective-permute-start | bytes 1572872 | tf_op jit(solution)/shard_map/ppermute | solution.py:40
  15.5 11.5 %collective-permute-done = bf16[128,2048]{1,0:T(8,128)(2,1)S(1)} collective-permute-done((bf16[128,2048]{1,0:T(8,128)(2,1)}, bf16[128,2048]{1,0:T(8,128)(2,1)S(1)}, u32[]{:S(2)}, u32[]{:S(2)}) %collective-permute-start) | collective-permute-done | bytes 524320 | tf_op jit(solution)/shard_map/ppermute | solution.py:40
  27.0 5.1 collective-permute-start.1
  32.1 10.3 %collective-permute-done.1 = bf16[128,2048]{1,0:T(8,128)(2,1)S(1)} collective-permute-done((bf16[128,2048]{1,0:T(8,128)(2,1)S(1)}, bf16[128,2048]{1,0:T(8,128)(2,1)S(1)}, u32[]{:S(2)}, u32[]{:S(2)}) %collective-permute-start.1) | collective-permute-done | bytes 524320 | tf_op jit(solution)/shard_map/ppermute | solution.py:40
  42.4 5.2 collective-permute-start.2
  47.6 19.0 %collective-permute-done.2 = bf16[128,2048]{1,0:T(8,128)(2,1)S(1)} collective-permute-done((bf16[128,2048]{1,0:T(8,128)(2,1)S(1)}, bf16[128,2048]{1,0:T(8,128)(2,1)S(1)}, u32[]{:S(2)}, u32[]{:S(2)}) %collective-permute-start.2) | collective-permute-done | bytes 524320 | tf_op jit(solution)/shard_map/ppermute | solution.py:40
  66.6 5.2 collective-permute-start.3
  71.8 12.8 %collective-permute-done.3 = bf16[128,2048]{1,0:T(8,128)(2,1)S(1)} collective-permute-done((bf16[128,2048]{1,0:T(8,128)(2,1)S(1)}, bf16[128,2048]{1,0:T(8,128)(2,1)S(1)}, u32[]{:S(2)}, u32[]{:S(2)}) %collective-permute-start.3) | collective-permute-done | bytes 524320 | tf_op jit(solution)/shard_map/ppermute | solution.py:40
  84.6 5.2 collective-permute-start.4
  89.8 1.9 constant_dynamic-update-slice_fusion.15
  91.7 19.7 %collective-permute-done.4 = bf16[128,2048]{1,0:T(8,128)(2,1)S(1)} collective-permute-done((bf16[128,2048]{1,0:T(8,128)(2,1)S(1)}, bf16[128,2048]{1,0:T(8,128)(2,1)S(1)}, u32[]{:S(2)}, u32[]{:S(2)}) %collective-permute-start.4) | collective-permute-done | bytes 524320 | tf_op jit(solution)/shard_map/ppermute | solution.py:40
  111.4 5.2 collective-permute-start.5
  116.6 0.8 constant_dynamic-update-slice_fusion.14
  117.4 0.8 constant_dynamic-update-slice_fusion.13
  118.2 0.8 constant_dynamic-update-slice_fusion.12
  119.1 19.2 %collective-permute-done.5 = bf16[128,2048]{1,0:T(8,128)(2,1)S(1)} collective-permute-done((bf16[128,2048]{1,0:T(8,128)(2,1)S(1)}, bf16[128,2048]{1,0:T(8,128)(2,1)S(1)}, u32[]{:S(2)}, u32[]{:S(2)}) %collective-permute-start.5) | collective-permute-done | bytes 524320 | tf_op jit(solution)/shard_map/ppermute | solution.py:40
  138.3 5.2 collective-permute-start.6
  143.5 0.8 constant_dynamic-update-slice_fusion.11
  144.3 0.8 constant_dynamic-update-slice_fusion.10
  145.2 0.9 constant_dynamic-update-slice_fusion.9
  146.0 10.1 %collective-permute-done.6 = bf16[128,2048]{1,0:T(8,128)(2,1)S(1)} collective-permute-done((bf16[128,2048]{1,0:T(8,128)(2,1)S(1)}, bf16[128,2048]{1,0:T(8,128)(2,1)S(1)}, u32[]{:S(2)}, u32[]{:S(2)}) %collective-permute-start.6) | collective-permute-done | bytes 524320 | tf_op jit(solution)/shard_map/ppermute | solution.py:40
  156.1 0.8 constant_dynamic-update-slice_fusion.8
  157.0 0.0 copy-done.1
  157.0 0.8 constant_dynamic-update-slice_fusion.7
  157.8 0.8 constant_dynamic-update-slice_fusion.6
  158.7 0.9 constant_dynamic-update-slice_fusion.5
  159.5 0.8 constant_dynamic-update-slice_fusion.4
  160.3 0.8 constant_dynamic-update-slice_fusion.3
  161.2 0.8 constant_dynamic-update-slice_fusion.2
  162.0 0.8 constant_dynamic-update-slice_fusion.1
  162.8 0.9 constant_dynamic-update-slice_fusion
  163.7 6.8 %fusion.3 = f32[2048,512]{1,0:T(8,128)} fusion(bf16[512,1024]{1,0:T(8,128)(2,1)} %all-gather.4.cloned.1.call-done, bf16[2048,2048]{1,0:T(8,128)(2,1)} %constant_dynamic-update-slice_fusion, s32[]{:T(128)S(6)} %select_n.14), kind=kOutput, calls=%fused_computation.8 | convolution fusion | flops 2147483648 | bytes 9437188 | tf_op jit(solution)/shard_map/dot_general | solution.py:44
  170.5 8.1 %multiply_bitcast_fusion = f32[1024,2048]{0,1:T(8,128)} fusion(bf16[512,1024]{1,0:T(8,128)(2,1)} %all-gather.6.cloned.1.call-done, f32[2048,512]{1,0:T(8,128)} %fusion.3), kind=kOutput, calls=%fused_computation.1 | convolution fusion | flops 2152726528 | bytes 13631488 | tf_op jit(solution)/shard_map/dot_general | solution.py:21
  178.7 6.0 %fusion = bf16[512,2048]{0,1:T(8,128)(2,1)S(1)} fusion(f32[2048,512]{1,0:T(8,128)} %fusion.3, bf16[512,1024]{1,0:T(8,128)(2,1)S(1)} %copy-done.2, bf16[2048,1024]{1,0:T(8,128)(2,1)} %all-gather.8.cloned.1.call-done), kind=kOutput, calls=%fused_computation.4 | convolution fusion | flops 2151677952 | bytes 11534336 | tf_op jit(solution)/shard_map/dot_general | solution.py:21
  184.7 0.0 copy-start.4
  184.7 1.3 copy-done.4
  186.1 2.4 multiply_bitcast_fusion.1
  188.5 1.0 copy-done
  189.4 6.4 %pad_maximum_fusion = f32[1024,4096]{0,1:T(8,128)} fusion(f32[1024,2048]{0,1:T(8,128)S(1)} %copy-done, f32[1024,2048]{0,1:T(8,128)S(1)} %multiply_bitcast_fusion.1), kind=kLoop, calls=%fused_computation | loop fusion | flops 4194304 | bytes 33554432 | tf_op jit(solution)/shard_map/concatenate | solution.py:71
  195.8 0.0 reduce-scatter.5.cloned.1.call-update
  195.8 0.2 reduce-scatter.3.cloned.1.call-start
  196.1 1.3 copy-done.5
  197.4 5.9 fusion.1
  203.3 0.0 reduce-scatter.3.cloned.1.call-update
  203.3 0.0 all-reduce.2.cloned.1.call-start
  203.4 275.0 %reduce-scatter.5.cloned.1.call-done = f32[128,4096]{0,1:T(8,128)} async-done(((f32[1024,4096]{0,1:T(8,128)}), f32[128,4096]{0,1:T(8,128)}) %reduce-scatter.5.cloned.1.call-update) | async-done | bytes 2097168 | tf_op jit(solution)/shard_map/reduce_scatter | solution.py:17
  478.4 0.0 all-reduce.2.cloned.1.call-update
  478.4 11.0 %reduce-scatter.3.cloned.1.call-done = f32[256,1024]{1,0:T(8,128)} async-done(((f32[512,1024]{1,0:T(8,128)}), f32[256,1024]{1,0:T(8,128)}) %reduce-scatter.3.cloned.1.call-update) | async-done | bytes 1048592 | tf_op jit(solution)/shard_map/reduce_scatter | solution.py:17
  489.4 2.1 convert_element_type.11
  491.4 64.3 %all-reduce.2.cloned.1.call-done = f32[128,4096]{0,1:T(8,128)} async-done(((f32[128,4096]{0,1:T(8,128)}), f32[128,4096]{0,1:T(8,128)}) %all-reduce.2.cloned.1.call-update) | async-done | bytes 2097168 | tf_op jit(solution)/shard_map/psum | solution.py:74
  555.8 2.4 multiply_reduce_fusion
  558.2 21.7 %psum.23 = f32[2048]{0:T(1024)S(1)} all-reduce(f32[2048]{0:T(1024)S(1)} %get-tuple-element.10), channel_id=1, replica_groups=mesh['rep'=2,'fs'=8,'tp'=2] {'fs'}, use_global_device_ids=true, to_apply=%region_6.7 | all-reduce | flops 2048 | bytes 16384 | tf_op jit(solution)/shard_map/psum | solution.py:79
  579.9 0.6 broadcast_multiply_fusion
  580.5 1.5 multiply_reduce_fusion.1
  582.0 2.5 psum.22
  584.4 0.5 broadcast_multiply_fusion.1
  584.9 1.3 copy.10
  (10 shorter events, 0.0 us)
Async XLA Ops:
  7.2 149.8 %copy-start.1 = (bf16[128,2048]{1,0:T(8,128)(2,1)S(1)}, bf16[128,2048]{1,0:T(8,128)(2,1)}, u32[]{:S(2)}) copy-start(bf16[128,2048]{1,0:T(8,128)(2,1)} %param.5) | copy-start | bytes 1572868
  7.2 156.6 %all-gather.4.cloned.1.call-start = ((), (), s32[]{:S(2)}) async-start(), calls=%async_computation.2 | async-start | bytes 1572864 | tf_op jit(solution)/shard_map/all_gather | solution.py:31
  7.9 162.6 %all-gather.6.cloned.1.call-start = ((), (), s32[]{:S(2)}) async-start(), calls=%async_computation.3 | async-start | bytes 1572864 | tf_op jit(solution)/shard_map/all_gather | solution.py:32
  8.7 170.0 %all-gather.8.cloned.1.call-start = ((), (), s32[]{:S(2)}) async-start(), calls=%async_computation.4 | async-start | bytes 4718592 | tf_op jit(solution)/shard_map/all_gather | solution.py:11
  9.4 469.0 %reduce-scatter.5.cloned.1.call-start = ((), (), s32[]{:S(2)}) async-start(), calls=%async_computation.6 | async-start | bytes 18874368 | tf_op jit(solution)/shard_map/reduce_scatter | solution.py:17
  9.4 17.6 %collective-permute-start = (bf16[128,2048]{1,0:T(8,128)(2,1)}, bf16[128,2048]{1,0:T(8,128)(2,1)S(1)}, u32[]{:S(2)}, u32[]{:S(2)}) collective-permute-start(bf16[128,2048]{1,0:T(8,128)(2,1)} %param.5), channel_id=1, source_target_pairs={{0,14},{2,0},{4,2},{6,4},{8,6},{10,8},{12,10},{14,12},{1,15},{3,1}... | collective-permute-start | bytes 1572872 | tf_op jit(solution)/shard_map/ppermute | solution.py:40
  27.0 15.4 %collective-permute-start.1 = (bf16[128,2048]{1,0:T(8,128)(2,1)S(1)}, bf16[128,2048]{1,0:T(8,128)(2,1)S(1)}, u32[]{:S(2)}, u32[]{:S(2)}) collective-permute-start(bf16[128,2048]{1,0:T(8,128)(2,1)S(1)} %collective-permute-done), channel_id=1, source_target_pairs={{0,14},{2,0},{4,2},{6,4},{8,6},{10,8},{12,10},{14,12},{1,15},{3,1}... | collective-permute-start | bytes 1572872 | tf_op jit(solution)/shard_map/ppermute | solution.py:40
  42.4 24.1 %collective-permute-start.2 = (bf16[128,2048]{1,0:T(8,128)(2,1)S(1)}, bf16[128,2048]{1,0:T(8,128)(2,1)S(1)}, u32[]{:S(2)}, u32[]{:S(2)}) collective-permute-start(bf16[128,2048]{1,0:T(8,128)(2,1)S(1)} %collective-permute-done.1), channel_id=1, source_target_pairs={{0,14},{2,0},{4,2},{6,4},{8,6},{10,8},{12,10},{14,12},{1,15},{3,1}... | collective-permute-start | bytes 1572872 | tf_op jit(solution)/shard_map/ppermute | solution.py:40
  66.6 18.0 %collective-permute-start.3 = (bf16[128,2048]{1,0:T(8,128)(2,1)S(1)}, bf16[128,2048]{1,0:T(8,128)(2,1)S(1)}, u32[]{:S(2)}, u32[]{:S(2)}) collective-permute-start(bf16[128,2048]{1,0:T(8,128)(2,1)S(1)} %collective-permute-done.2), channel_id=1, source_target_pairs={{0,14},{2,0},{4,2},{6,4},{8,6},{10,8},{12,10},{14,12},{1,15},{3,1}... | collective-permute-start | bytes 1572872 | tf_op jit(solution)/shard_map/ppermute | solution.py:40
  84.6 26.8 %collective-permute-start.4 = (bf16[128,2048]{1,0:T(8,128)(2,1)S(1)}, bf16[128,2048]{1,0:T(8,128)(2,1)S(1)}, u32[]{:S(2)}, u32[]{:S(2)}) collective-permute-start(bf16[128,2048]{1,0:T(8,128)(2,1)S(1)} %collective-permute-done.3), channel_id=1, source_target_pairs={{0,14},{2,0},{4,2},{6,4},{8,6},{10,8},{12,10},{14,12},{1,15},{3,1}... | collective-permute-start | bytes 1572872 | tf_op jit(solution)/shard_map/ppermute | solution.py:40
  111.4 26.9 %collective-permute-start.5 = (bf16[128,2048]{1,0:T(8,128)(2,1)S(1)}, bf16[128,2048]{1,0:T(8,128)(2,1)S(1)}, u32[]{:S(2)}, u32[]{:S(2)}) collective-permute-start(bf16[128,2048]{1,0:T(8,128)(2,1)S(1)} %collective-permute-done.4), channel_id=1, source_target_pairs={{0,14},{2,0},{4,2},{6,4},{8,6},{10,8},{12,10},{14,12},{1,15},{3,1}... | collective-permute-start | bytes 1572872 | tf_op jit(solution)/shard_map/ppermute | solution.py:40
  138.3 17.8 %collective-permute-start.6 = (bf16[128,2048]{1,0:T(8,128)(2,1)S(1)}, bf16[128,2048]{1,0:T(8,128)(2,1)S(1)}, u32[]{:S(2)}, u32[]{:S(2)}) collective-permute-start(bf16[128,2048]{1,0:T(8,128)(2,1)S(1)} %collective-permute-done.5), channel_id=1, source_target_pairs={{0,14},{2,0},{4,2},{6,4},{8,6},{10,8},{12,10},{14,12},{1,15},{3,1}... | collective-permute-start | bytes 1572872 | tf_op jit(solution)/shard_map/ppermute | solution.py:40
  170.5 8.1 %copy-start.2 = (bf16[512,1024]{1,0:T(8,128)(2,1)S(1)}, bf16[512,1024]{1,0:T(8,128)(2,1)}, u32[]{:S(2)}) copy-start(bf16[512,1024]{1,0:T(8,128)(2,1)} %all-gather.6.cloned.1.call-done) | copy-start | bytes 3145732
  178.7 7.4 %copy-start.3 = (bf16[512,1024]{1,0:T(8,128)(2,1)S(1)}, bf16[512,1024]{1,0:T(8,128)(2,1)}, u32[]{:S(2)}) copy-start(bf16[512,1024]{1,0:T(8,128)(2,1)} %all-gather.4.cloned.1.call-done) | copy-start | bytes 3145732
  184.7 1.3 copy-start.4
  186.1 3.4 copy-start
  195.8 1.6 copy-start.5
  195.8 293.5 %reduce-scatter.3.cloned.1.call-start = ((), (), s32[]{:S(2)}) async-start(), calls=%async_computation.5 | async-start | bytes 3145728 | tf_op jit(solution)/shard_map/reduce_scatter | solution.py:17
  203.3 352.5 %all-reduce.2.cloned.1.call-start = ((), (), s32[]{:S(2)}) async-start(), calls=%async_computation.7 | async-start | bytes 4194304 | tf_op jit(solution)/shard_map/psum | solution.py:74
Sparse Core Ops, SparseCore 0:
  9.5 11.7 all-gather.3
  22.9 10.1 all-gather.5
  35.1 114.6 all-gather.7
  196.0 282.3 reduce-scatter.4
  480.5 8.8 reduce-scatter.2
  491.5 64.2 all-reduce.1
